TPU v7x, 32 devices: a whole 2x2x4 slice. The times are simulated.
32 devices in a mesh: fs: 8 (over z, x), tp: 4 (over y, core).
Axes of the slice: x: 2, y: 2, z: 4, core: 2. Of those that a mesh axis runs over, the one named last changes fastest.
Arguments:
- layer_input: bfloat16 [6144, 2048], P('fs'), may hold values from -6 to 6
- branch_cotangent: bfloat16 [6144, 1024], P('fs', 'tp'), may hold values from -0.057373047 to 0.057373047
- gate_cotangent: bfloat16 [6144, 1024], P('fs', 'tp'), may hold values from -0.057373047 to 0.057373047
- branch_factor: bfloat16 [2048, 128], P('fs'), may hold values from -0.5 to 0.5
- gate_factor: bfloat16 [2048, 128], P('fs'), may hold values from -0.5 to 0.5
- branch_weight: float32 [2048, 1024], P('fs', 'tp'), may hold values from -6 to 6
- gate_weight: float32 [2048, 1024], P('fs', 'tp'), may hold values from -6 to 6
- branch_first: float32 [128, 1024], P(None, 'tp'), may hold values from -6 to 6
- gate_first: float32 [128, 1024], P(None, 'tp'), may hold values from -6 to 6
- branch_second: float32 [128, 1024], P(None, 'tp'), may hold values from 0.0625 to 900
- gate_second: float32 [128, 1024], P(None, 'tp'), may hold values from 0.0625 to 900
Outputs:
- branch_step: float32 [2048, 1024], P('fs', 'tp')
- gate_step: float32 [2048, 1024], P('fs', 'tp')
- branch_new: float32 [2048, 1024], P('fs', 'tp')
- gate_new: float32 [2048, 1024], P('fs', 'tp')
- branch_copy: bfloat16 [2048, 1024], P(None, 'tp')
- gate_copy: bfloat16 [2048, 1024], P(None, 'tp')
- branch_first_new: float32 [128, 1024], P(None, 'tp')
- gate_first_new: float32 [128, 1024], P(None, 'tp')
- branch_second_new: float32 [128, 1024], P(None, 'tp')
- gate_second_new: float32 [128, 1024], P(None, 'tp')
All inputs are finite; a program needn't handle non-finite values.
Results may differ from a plain program's by a relative error of at most 0.00055.
Values may be sent and summed in bfloat16 or wider, within the bound.
A program may use at most 64 MiB of HBM per device.

v0:
```python
import jax
import jax.numpy as jnp
from jax import lax
from jax.sharding import PartitionSpec as P

first_decay = 0.8
second_decay = 0.9
learn_rate = 0.5


def update_moments(projected, first_old, second_old):
    first_new = first_decay * first_old + (1.0 - first_decay) * projected
    second_new = second_decay * second_old + (1.0 - second_decay) * projected * projected
    return (first_new, second_new, first_new / jnp.sqrt(second_new))


def local(
    layer_input,
    branch_cotangent,
    gate_cotangent,
    branch_factor,
    gate_factor,
    branch_weight,
    gate_weight,
    branch_first,
    gate_first,
    branch_second,
    gate_second,
):
    highest = lax.Precision.HIGHEST
    width = branch_cotangent.shape[1]
    branch_whole, gate_whole = (
        lax.all_gather(branch_factor, "fs", axis=0, tiled=True),
        lax.all_gather(gate_factor, "fs", axis=0, tiled=True),
    )
    branch_rows = jnp.dot(layer_input, branch_whole, preferred_element_type=jnp.float32)
    gate_rows = jnp.dot(layer_input, gate_whole, preferred_element_type=jnp.float32)
    branch_local = jnp.einsum(
        "tr,tw->rw", branch_rows, branch_cotangent.astype(jnp.float32), precision=highest
    )
    gate_local = jnp.einsum(
        "tr,tw->rw", gate_rows, gate_cotangent.astype(jnp.float32), precision=highest
    )
    branch_projected, gate_projected = lax.psum((branch_local, gate_local), "fs")
    branch_first_new, branch_second_new, branch_direction = update_moments(
        branch_projected, branch_first, branch_second
    )
    gate_first_new, gate_second_new, gate_direction = update_moments(
        gate_projected, gate_first, gate_second
    )
    local_squares = jnp.sum(branch_direction * branch_direction) + jnp.sum(
        gate_direction * gate_direction
    )
    sum_squares = lax.psum(local_squares, "tp")
    entries = 2 * branch_direction.shape[0] * width * lax.axis_size("tp")
    step_scale = learn_rate / jnp.sqrt(sum_squares / entries + 1e-06)
    branch_step = -step_scale * jnp.dot(
        branch_factor.astype(jnp.float32), branch_direction, precision=highest
    )
    gate_step = -step_scale * jnp.dot(
        gate_factor.astype(jnp.float32), gate_direction, precision=highest
    )
    branch_new = branch_weight + branch_step
    gate_new = gate_weight + gate_step
    branch_copy, gate_copy = (
        lax.all_gather(branch_new.astype(jnp.bfloat16), "fs", axis=0, tiled=True),
        lax.all_gather(gate_new.astype(jnp.bfloat16), "fs", axis=0, tiled=True),
    )
    return (
        branch_step,
        gate_step,
        branch_new,
        gate_new,
        branch_copy,
        gate_copy,
        branch_first_new,
        gate_first_new,
        branch_second_new,
        gate_second_new,
    )


def solution(mesh):
    return jax.shard_map(
        local,
        mesh=mesh,
        in_specs=(
            P("fs", None),
            P("fs", "tp"),
            P("fs", "tp"),
            P("fs", None),
            P("fs", None),
            P("fs", "tp"),
            P("fs", "tp"),
            P(None, "tp"),
            P(None, "tp"),
            P(None, "tp"),
            P(None, "tp"),
        ),
        out_specs=(
            P("fs", "tp"),
            P("fs", "tp"),
            P("fs", "tp"),
            P("fs", "tp"),
            P(None, "tp"),
            P(None, "tp"),
            P(None, "tp"),
            P(None, "tp"),
            P(None, "tp"),
            P(None, "tp"),
        ),
        check_vma=False,
    )
```

profile of v0, /device:TPU:0, one launch (start us, length us, event | category | flops | bytes accessed | tf_op | source)
XLA Modules:
  0.0 251.8 jit_solution(14178861783154490260)
XLA Ops:
  7.2 0.0 copy-start
  7.2 0.0 all-reduce.3.cloned.1.call-start
  7.2 33.4 %all_gather.12 = bf16[2048,128]{1,0:T(8,128)(2,1)S(1)} all-gather(bf16[256,128]{1,0:T(8,128)(2,1)} %param.14), channel_id=1, replica_groups=mesh['fs'=8,'tp'=4] {'fs'}, dimensions={0}, use_global_device_ids=true | all-gather | bytes 589824 | tf_op jit(solution)/shard_map/all_gather | solution.py:33
  40.6 31.4 %all_gather.13 = bf16[2048,128]{1,0:T(8,128)(2,1)S(1)} all-gather(bf16[256,128]{1,0:T(8,128)(2,1)} %param.15), channel_id=1, replica_groups=mesh['fs'=8,'tp'=4] {'fs'}, dimensions={0}, use_global_device_ids=true | all-gather | bytes 589824 | tf_op jit(solution)/shard_map/all_gather | solution.py:34
  72.0 0.0 copy-done
  72.0 1.0 fusion.8
  73.0 0.0 copy-start.2
  73.0 0.0 copy-start.3
  73.0 0.0 copy-start.4
  73.0 1.0 fusion.10
  74.0 0.0 copy-done.2
  74.0 1.1 fusion.9
  75.2 0.0 copy-done.3
  75.2 1.1 fusion.11
  76.3 0.0 all-reduce.3.cloned.1.call-update
  76.3 0.0 all-gather.5.cloned.1.call-start
  76.4 72.8 %all-reduce.3.cloned.1.call-done = (f32[128,256]{1,0:T(8,128)}, f32[128,256]{1,0:T(8,128)}) async-done(((f32[128,256]{1,0:T(8,128)}, f32[128,256]{1,0:T(8,128)}), (f32[128,256]{1,0:T(8,128)}, f32[128,256]{1,0:T(8,128)})) %all-reduce.3.cloned.1.call-update) | async-done | bytes 262160 | tf_op jit(solution)/shard_map/psum | solution.py:44
  149.1 2.6 %multiply_reduce_fusion = (f32[]{:T(128)}, f32[128,256]{1,0:T(8,128)S(1)}, f32[128,256]{1,0:T(8,128)}, f32[]{:T(128)}, f32[128,256]{1,0:T(8,128)}, /*index=5*/f32[128,256]{1,0:T(8,128)}) fusion(f32[128,256]{1,0:T(8,128)} %get-tuple-element.21, f32[128,256]{1,0:T(8,128)} %param.21, f32[128,256]{1,0:T(8,128)} %param.19, f32[128,256]{1,0:T(8,128)} %get-tuple-element.20, ...), kind=kLoop, calls=%fused_computation.8 | loop fusion | flops 655358 | bytes 1310728 | tf_op jit(solution)/shard_map/reduce_sum | solution.py:51
  151.7 0.0 copy-start.1
  153.0 0.0 copy-done.4
  153.1 0.8 copy.22
  153.9 6.1 %psum.23 = f32[]{:T(128)} all-reduce(f32[]{:T(128)S(6)} %add.34), channel_id=1, replica_groups=mesh['fs'=8,'tp'=4] {'tp'}, use_global_device_ids=true, to_apply=%region_4.0 | all-reduce | flops 1 | bytes 8 | tf_op jit(solution)/shard_map/psum | solution.py:54
  160.7 2.1 fusion.4
  162.8 0.0 all-gather.5.cloned.1.call-update
  162.9 0.0 all-gather.3.cloned.1.call-start
  162.9 1.8 copy.21
  164.7 2.3 fusion.5
  167.0 0.0 all-gather.3.cloned.1.call-update
  167.0 1.8 copy.26
  168.8 0.8 copy.24
  169.6 1.8 copy.25
  171.4 1.8 copy.23
  173.2 28.7 %all-gather.5.cloned.1.call-done = bf16[2048,256]{0,1:T(8,128)(2,1)} async-done(((bf16[256,256]{0,1:T(8,128)(2,1)}), bf16[2048,256]{0,1:T(8,128)(2,1)}) %all-gather.5.cloned.1.call-update) | async-done | bytes 1048592 | tf_op jit(solution)/shard_map/all_gather | solution.py:67
  201.9 2.3 copy.28
  204.2 0.0 copy-done.1
  204.2 38.8 %all-gather.3.cloned.1.call-done = bf16[2048,256]{0,1:T(8,128)(2,1)} async-done(((bf16[256,256]{0,1:T(8,128)(2,1)}), bf16[2048,256]{0,1:T(8,128)(2,1)}) %all-gather.3.cloned.1.call-update) | async-done | bytes 1048592 | tf_op jit(solution)/shard_map/all_gather | solution.py:66
  243.0 2.3 copy.27
Async XLA Ops:
  7.2 64.8 %copy-start = (bf16[768,2048]{1,0:T(8,128)(2,1)S(1)}, bf16[768,2048]{1,0:T(8,128)(2,1)}, u32[]{:S(2)}) copy-start(bf16[768,2048]{1,0:T(8,128)(2,1)} %param.11) | copy-start | bytes 9437188
  7.2 142.0 %all-reduce.3.cloned.1.call-start = ((), (), s32[]{:S(2)}) async-start(), calls=%async_computation.2 | async-start | bytes 524288 | tf_op jit(solution)/shard_map/psum | solution.py:44
  73.0 1.0 copy-start.2
  73.0 2.2 copy-start.3
  73.0 80.0 %copy-start.4 = (f32[256,256]{1,0:T(8,128)S(1)}, f32[256,256]{1,0:T(8,128)}, u32[]{:S(2)}) copy-start(f32[256,256]{1,0:T(8,128)} %param.17) | copy-start | bytes 786436
  76.3 125.6 %all-gather.5.cloned.1.call-start = ((), (), s32[]{:S(2)}) async-start(), calls=%async_computation.1 | async-start | bytes 1179648 | tf_op jit(solution)/shard_map/all_gather | solution.py:67
  151.7 52.4 %copy-start.1 = (f32[128,256]{1,0:T(8,128)}, f32[128,256]{1,0:T(8,128)S(1)}, u32[]{:S(2)}) copy-start(f32[128,256]{1,0:T(8,128)S(1)} %get-tuple-element.27) | copy-start | bytes 393220
  162.9 80.1 %all-gather.3.cloned.1.call-start = ((), (), s32[]{:S(2)}) async-start(), calls=%async_computation | async-start | bytes 1179648 | tf_op jit(solution)/shard_map/all_gather | solution.py:66
Sparse Core Ops, SparseCore 0:
  76.5 72.6 all-reduce.2
  163.0 38.8 all-gather.4
  204.5 38.3 all-gather.2
where the time goes:
time: 252 us
  waiting for transfers between devices  140 us (56%)
  blocking collectives  70.9 us (28%)
  between operations  15.8 us (6%)
  local copies, waits for them, and re-layouts  13.4 us (5%)
  matrix products  8.61 us (3%)
  other arithmetic  2.6 us (1%)
    psum x1, waiting for transfers between devices, local(): lax.psum((branch_local, gate_local), 'fs')  72.8 us
    all_gather x1, waiting for transfers between devices, local(): lax.all_gather(branch_new.astype(jnp.bfloat16), 'fs', axis=0, tiled=True)  38.8 us
    all_gather x1, blocking collectives, local(): lax.all_gather(branch_factor, 'fs', axis=0, tiled=True)  33.4 us
    all_gather x1, blocking collectives, local(): lax.all_gather(gate_factor, 'fs', axis=0, tiled=True)  31.4 us
    all_gather x1, waiting for transfers between devices, local(): lax.all_gather(gate_new.astype(jnp.bfloat16), 'fs', axis=0, tiled=True)  28.7 us
    unnamed x18, local copies, waits for them, and re-layouts  13.4 us
    psum x1, blocking collectives, local(): sum_squares = lax.psum(local_squares, 'tp')  6.14 us
  transfers between devices with their start and end apart: 3, of which 3 were waited for; matrix products, arithmetic and copies ran while one was open for 5% of the time, Pallas kernels for 0%

commit v1 on v0

--- a/solution.py
+++ b/solution.py
@@ -27,10 +27,18 @@
     branch_second,
     gate_second,
 ):
+
+    def lead_regions(work_x):
+        answer = jax.lax.psum(1, "fs")
+        new = jnp.stack([work_x] * answer, axis=0)
+        reached = jax.lax.all_to_all(new, "fs", 0, 0)
+        taken_in = jnp.concatenate(reached, axis=0)
+        return taken_in
+
     highest = lax.Precision.HIGHEST
     width = branch_cotangent.shape[1]
     branch_whole, gate_whole = (
-        lax.all_gather(branch_factor, "fs", axis=0, tiled=True),
+        lead_regions(branch_factor),
         lax.all_gather(gate_factor, "fs", axis=0, tiled=True),
     )
     branch_rows = jnp.dot(layer_input, branch_whole, preferred_element_type=jnp.float32)

time: 252 us -> 233 us (0.925)
  blocking collectives: 70.9 us -> 44.7 us
  starting transfers between devices: 0.12 us -> 7.41 us
  waiting for transfers between devices: 140 us -> 136 us
  local copies, waits for them, and re-layouts: 13.4 us -> 16.2 us
    all_gather x1 -> x0, blocking collectives: 33.4 us -> none  [local(): lax.all_gather(branch_factor, 'fs', axis=0, tiled=True)]
    all_to_all x0 -> x1, starting transfers between devices: none -> 7.28 us  [lead_regions(): reached = jax.lax.all_to_all(new, 'fs', 0, 0)]
    all_gather x1, blocking collectives: 31.4 us -> 38.5 us  [local(): lax.all_gather(gate_factor, 'fs', axis=0, tiled=True)]
    psum x1, waiting for transfers between devices: 72.8 us -> 68.7 us  [local(): lax.psum((branch_local, gate_local), 'fs')]
    unnamed x18 -> x16, local copies, waits for them, and re-layouts: 13.4 us -> 14.3 us
  transfers between devices with their start and end apart: 3 -> 4, of which waited for: 3 -> 3; matrix products, arithmetic and copies ran while one was open for 5% -> 6% of each run, Pallas kernels for 0% -> 0%
where the time goes in v1:
time: 233 us
  waiting for transfers between devices  136 us (58%)
  blocking collectives  44.7 us (19%)
  local copies, waits for them, and re-layouts  16.2 us (7%)
  between operations  15.8 us (7%)
  matrix products  9.71 us (4%)
  starting transfers between devices  7.41 us (3%)
  other arithmetic  2.6 us (1%)
    psum x1, waiting for transfers between devices, local(): lax.psum((branch_local, gate_local), 'fs')  68.7 us
    all_gather x1, waiting for transfers between devices, local(): lax.all_gather(branch_new.astype(jnp.bfloat16), 'fs', axis=0, tiled=True)  38.8 us
    all_gather x1, blocking collectives, local(): lax.all_gather(gate_factor, 'fs', axis=0, tiled=True)  38.5 us
    all_gather x1, waiting for transfers between devices, local(): lax.all_gather(gate_new.astype(jnp.bfloat16), 'fs', axis=0, tiled=True)  28.7 us
    unnamed x16, local copies, waits for them, and re-layouts  14.3 us
    all_to_all x1, starting transfers between devices, lead_regions(): reached = jax.lax.all_to_all(new, 'fs', 0, 0)  7.28 us
    psum x1, blocking collectives, local(): sum_squares = lax.psum(local_squares, 'tp')  6.14 us
  transfers between devices with their start and end apart: 4, of which 3 were waited for; matrix products, arithmetic and copies ran while one was open for 6% of the time, Pallas kernels for 0%

profile of v1, /device:TPU:0, one launch (start us, length us, event | category | flops | bytes accessed | tf_op | source)
XLA Modules:
  0.0 232.6 jit_solution(5471260114349986773)
XLA Ops:
  7.2 0.0 copy-start
  7.2 1.9 stack.2
  9.0 7.3 %all-to-all-start = ((bf16[8,256,128]{2,1,0:T(8,128)(2,1)}), bf16[8,256,128]{2,1,0:T(8,128)(2,1)}, u32[]{:S(2)}, u32[]{:S(2)}) async-start(bf16[8,256,128]{2,1,0:T(8,128)(2,1)} %stack.2), calls=%async_computation | async-start | bytes 1048576 | tf_op jit(solution)/shard_map/all_to_all | solution.py:34
  16.3 0.0 copy-start.2
  16.3 0.0 all-reduce.3.cloned.1.call-start
  16.4 38.5 %all_gather.9 = bf16[2048,128]{1,0:T(8,128)(2,1)S(1)} all-gather(bf16[256,128]{1,0:T(8,128)(2,1)} %param.15), channel_id=1, replica_groups=mesh['fs'=8,'tp'=4] {'fs'}, dimensions={0}, use_global_device_ids=true | all-gather | bytes 589824 | tf_op jit(solution)/shard_map/all_gather | solution.py:42
  54.9 0.0 copy-done
  54.9 1.0 fusion.10
  55.9 0.0 copy-done.2
  55.9 1.1 fusion.11
  57.1 0.0 copy-start.3
  57.1 0.0 all-to-all-done
  57.1 2.1 fusion.8
  59.1 0.0 copy-done.3
  59.1 1.1 fusion.9
  60.3 0.0 all-reduce.3.cloned.1.call-update
  60.3 0.0 all-gather.5.cloned.1.call-start
  60.3 68.7 %all-reduce.3.cloned.1.call-done = (f32[128,256]{1,0:T(8,128)}, f32[128,256]{1,0:T(8,128)}) async-done(((f32[128,256]{1,0:T(8,128)}, f32[128,256]{1,0:T(8,128)}), (f32[128,256]{1,0:T(8,128)}, f32[128,256]{1,0:T(8,128)})) %all-reduce.3.cloned.1.call-update) | async-done | bytes 262160 | tf_op jit(solution)/shard_map/psum | solution.py:52
  129.1 2.6 %multiply_reduce_fusion = (f32[]{:T(128)}, f32[128,256]{1,0:T(8,128)S(1)}, f32[128,256]{1,0:T(8,128)}, f32[]{:T(128)}, f32[128,256]{1,0:T(8,128)}, /*index=5*/f32[128,256]{1,0:T(8,128)}) fusion(f32[128,256]{1,0:T(8,128)} %get-tuple-element.21, f32[128,256]{1,0:T(8,128)} %param.21, f32[128,256]{1,0:T(8,128)} %param.19, f32[128,256]{1,0:T(8,128)} %get-tuple-element.20, ...), kind=kLoop, calls=%fused_computation.8 | loop fusion | flops 655358 | bytes 1310728 | tf_op jit(solution)/shard_map/reduce_sum | solution.py:59
  131.7 0.0 copy-start.1
  133.0 1.8 copy.22
  134.7 6.1 %psum.23 = f32[]{:T(128)} all-reduce(f32[]{:T(128)S(6)} %add.34), channel_id=1, replica_groups=mesh['fs'=8,'tp'=4] {'tp'}, use_global_device_ids=true, to_apply=%region_4.0 | all-reduce | flops 1 | bytes 8 | tf_op jit(solution)/shard_map/psum | solution.py:62
  141.6 2.1 fusion.4
  143.7 0.0 all-gather.5.cloned.1.call-update
  143.7 0.0 all-gather.3.cloned.1.call-start
  143.8 1.8 copy.21
  145.6 2.3 fusion.5
  147.8 0.0 all-gather.3.cloned.1.call-update
  147.8 1.8 copy.26
  149.6 0.8 copy.24
  150.5 1.8 copy.25
  152.3 1.8 copy.23
  154.1 28.7 %all-gather.5.cloned.1.call-done = bf16[2048,256]{0,1:T(8,128)(2,1)} async-done(((bf16[256,256]{0,1:T(8,128)(2,1)}), bf16[2048,256]{0,1:T(8,128)(2,1)}) %all-gather.5.cloned.1.call-update) | async-done | bytes 1048592 | tf_op jit(solution)/shard_map/all_gather | solution.py:75
  182.8 2.3 copy.28
  185.0 0.0 copy-done.1
  185.0 38.8 %all-gather.3.cloned.1.call-done = bf16[2048,256]{0,1:T(8,128)(2,1)} async-done(((bf16[256,256]{0,1:T(8,128)(2,1)}), bf16[2048,256]{0,1:T(8,128)(2,1)}) %all-gather.3.cloned.1.call-update) | async-done | bytes 1048592 | tf_op jit(solution)/shard_map/all_gather | solution.py:74
  223.8 2.3 copy.27
Async XLA Ops:
  7.2 47.7 %copy-start = (bf16[768,2048]{1,0:T(8,128)(2,1)S(1)}, bf16[768,2048]{1,0:T(8,128)(2,1)}, u32[]{:S(2)}) copy-start(bf16[768,2048]{1,0:T(8,128)(2,1)} %param.11) | copy-start | bytes 9437188
  9.0 48.0 %all-to-all-start = ((bf16[8,256,128]{2,1,0:T(8,128)(2,1)}), bf16[8,256,128]{2,1,0:T(8,128)(2,1)}, u32[]{:S(2)}, u32[]{:S(2)}) async-start(bf16[8,256,128]{2,1,0:T(8,128)(2,1)} %stack.2), calls=%async_computation | async-start | bytes 1048576 | tf_op jit(solution)/shard_map/all_to_all | solution.py:34
  16.3 39.6 %copy-start.2 = (bf16[768,256]{1,0:T(8,128)(2,1)S(1)}, bf16[768,256]{1,0:T(8,128)(2,1)}, u32[]{:S(2)}) copy-start(bf16[768,256]{1,0:T(8,128)(2,1)} %param.13) | copy-start | bytes 1179652
  16.3 112.7 %all-reduce.3.cloned.1.call-start = ((), (), s32[]{:S(2)}) async-start(), calls=%async_computation.3 | async-start | bytes 524288 | tf_op jit(solution)/shard_map/psum | solution.py:52
  57.1 2.1 copy-start.3
  60.3 122.5 %all-gather.5.cloned.1.call-start = ((), (), s32[]{:S(2)}) async-start(), calls=%async_computation.2 | async-start | bytes 1179648 | tf_op jit(solution)/shard_map/all_gather | solution.py:75
  131.7 53.4 %copy-start.1 = (f32[128,256]{1,0:T(8,128)}, f32[128,256]{1,0:T(8,128)S(1)}, u32[]{:S(2)}) copy-start(f32[128,256]{1,0:T(8,128)S(1)} %get-tuple-element.27) | copy-start | bytes 393220
  143.7 80.1 %all-gather.3.cloned.1.call-start = ((), (), s32[]{:S(2)}) async-start(), calls=%async_computation.1 | async-start | bytes 1179648 | tf_op jit(solution)/shard_map/all_gather | solution.py:74
Sparse Core Ops, SparseCore 0:
  60.4 68.5 all-reduce.2
  143.8 38.8 all-gather.4
  185.4 38.3 all-gather.2
